TPU v7x, 32 devices: a whole 2x2x4 slice. The times are simulated.
32 devices in a mesh: ep: 4 (over y, x), tp: 8 (over z, core).
Axes of the slice: x: 2, y: 2, z: 4, core: 2. Of those that a mesh axis runs over, the one named last changes fastest.
Arguments:
- tokens: bfloat16 [64, 4096], P(None, 'ep'), may hold values from -60 to 60
- gain_attn: bfloat16 [4096], P('ep'), may hold values from 0.099609375 to 1.8984375
- w_query: bfloat16 [4096, 2048], P('ep', 'tp'), may hold values from -0.09375 to 0.09375
- w_key: bfloat16 [4096, 2048], P('ep', 'tp'), may hold values from -0.09375 to 0.09375
- w_value: bfloat16 [4096, 2048], P('ep', 'tp'), may hold values from -0.09375 to 0.09375
- w_output: bfloat16 [2048, 4096], P('tp', 'ep'), may hold values from -0.125 to 0.125
- key_cache: bfloat16 [64, 1024, 2048], P('ep', None, 'tp'), may hold values from -6 to 6
- value_cache: bfloat16 [64, 1024, 2048], P('ep', None, 'tp'), may hold values from -10 to 10
- lengths: int32 [64], P('ep'), may hold values from 128 to 1024
- score_shift: float32 [16], P('tp'), may hold values from -9.5 to -3.5
- gain_ffn: bfloat16 [4096], replicated, may hold values from 0.099609375 to 1.8984375
- w_mix: bfloat16 [4096], P('ep'), may hold values from -0.09375 to 0.09375
- w_dense_gate: bfloat16 [4096, 4096], P('ep', 'tp'), may hold values from -0.09375 to 0.09375
- w_dense_up: bfloat16 [4096, 4096], P('ep', 'tp'), may hold values from -0.09375 to 0.09375
- w_dense_down: bfloat16 [4096, 4096], P('tp', 'ep'), may hold values from -0.09375 to 0.09375
- route_group: int32 [64], replicated, may hold values from 0 to 3, as said below
- route_inner: int32 [64, 2], replicated, may hold values from 0 to 3, as said below
- route_weight: float32 [64, 2], replicated, may hold values from 0.3 to 1
- w_exp_gate: bfloat16 [16, 4096, 2048], P('ep', None, 'tp'), may hold values from -0.09375 to 0.09375
- w_exp_up: bfloat16 [16, 4096, 2048], P('ep', None, 'tp'), may hold values from -0.09375 to 0.09375
- w_exp_down: bfloat16 [16, 2048, 4096], P('ep', 'tp'), may hold values from -0.125 to 0.125
Outputs:
- mixed: bfloat16 [64, 4096], P(None, 'ep')
- new_keys: bfloat16 [64, 2048], P('ep', 'tp')
- new_values: bfloat16 [64, 2048], P('ep', 'tp')
Inputs may be any that keep to these rules, and one draw needn't show every extreme that they name: `route_group`: within every aligned block of 16 sequences (the sequences of one index of ep) exactly half of the tokens use one group, the same group in every block; the other groups share the rest. A token's 2 experts inside its group differ. Within every aligned block of 16 sequences no expert (route_group * 4 + route_inner) is used by more than 4 tokens, and the experts of the group that half of the block uses are each used by exactly 4.
All inputs are finite; a program needn't handle non-finite values.
Results may differ from a plain program's by a relative error of at most 0.0039.
The roundings to bfloat16 on the way count: a program that leaves them out, or rounds other values in their place, can miss the bound.
Values may be sent and summed in bfloat16 or wider, within the bound.
A program may use at most 128 MiB of HBM per device.

v0:
```python
import math
import jax
import jax.numpy as jnp
from jax import lax
from jax.sharding import PartitionSpec as P

D = 4096
HD = 128
EPG = 4
TOPK = 2
EXPERTS = 16
CAP = 4
norm_eps = 1e-06


def on_device(
    tokens,
    gain_attn,
    w_query,
    w_key,
    w_value,
    w_output,
    key_cache,
    value_cache,
    lengths,
    score_shift,
    gain_ffn,
    w_mix,
    w_dense_gate,
    w_dense_up,
    w_dense_down,
    route_group,
    route_inner,
    route_weight,
    w_exp_gate,
    w_exp_up,
    w_exp_down,
):
    ep_count = lax.axis_size("ep")
    batch_all, col_width = tokens.shape
    seq_local = batch_all // ep_count
    head_cols = w_query.shape[1]
    heads_local = head_cols // HD
    tokens_float = tokens.astype(jnp.float32)
    squares = lax.psum_scatter(
        jnp.sum(tokens_float * tokens_float, axis=1), "ep", scatter_dimension=0, tiled=True
    )
    inv_first = lax.rsqrt(squares / D + norm_eps)[:, None]
    scaled_in = (tokens_float * gain_attn.astype(jnp.float32)).astype(jnp.bfloat16)
    w_joint = jnp.concatenate([w_query, w_key, w_value], axis=1)
    joint_proj = (
        lax.psum_scatter(
            jnp.dot(scaled_in, w_joint, preferred_element_type=jnp.float32),
            "ep",
            scatter_dimension=0,
            tiled=True,
        )
        * inv_first
    )
    queries = joint_proj[:, :head_cols].astype(jnp.bfloat16)
    new_keys = joint_proj[:, head_cols : 2 * head_cols].astype(jnp.bfloat16)
    new_values = joint_proj[:, 2 * head_cols :].astype(jnp.bfloat16)
    cache_len = key_cache.shape[1]
    head_query = queries.reshape(seq_local, heads_local, HD)
    head_keys = key_cache.reshape(seq_local, cache_len, heads_local, HD)
    scores = jnp.einsum(
        "bhd,blhd->bhl", head_query, head_keys, preferred_element_type=jnp.float32
    ) / math.sqrt(HD)
    scores = scores + score_shift[None, :, None]
    live_mask = lax.broadcasted_iota(jnp.int32, scores.shape, 2) < lengths[:, None, None]
    soft_terms = jnp.where(live_mask, jax.nn.softplus(scores), 0.0)
    later_sum = lax.cumsum(soft_terms, axis=2, reverse=True) - soft_terms
    stick = jnp.where(live_mask, jnp.exp(jax.nn.log_sigmoid(scores) - later_sum), 0.0).astype(
        jnp.bfloat16
    )
    head_values = value_cache.reshape(seq_local, cache_len, heads_local, HD)
    attended = jnp.einsum("bhl,blhd->bhd", stick, head_values, preferred_element_type=jnp.float32)
    attended = attended.reshape(seq_local, head_cols).astype(jnp.bfloat16)
    attn_part = jnp.dot(
        lax.all_gather(attended, "ep", axis=0, tiled=True),
        w_output,
        preferred_element_type=jnp.float32,
    )
    attn_out = lax.psum(attn_part, "tp")
    middle = (tokens_float + attn_out).astype(jnp.bfloat16)
    middle_float = middle.astype(jnp.float32)
    gain_float = gain_ffn.astype(jnp.float32)
    gain_cols = lax.dynamic_slice_in_dim(gain_float, lax.axis_index("ep") * col_width, col_width, 0)
    scaled_mid = (middle_float * gain_cols).astype(jnp.bfloat16)
    dense_pre, dense_lin, mix_pre, mid_squares = lax.psum(
        (
            jnp.dot(scaled_mid, w_dense_gate, preferred_element_type=jnp.float32),
            jnp.dot(scaled_mid, w_dense_up, preferred_element_type=jnp.float32),
            jnp.dot(scaled_mid, w_mix, preferred_element_type=jnp.float32),
            jnp.sum(middle_float * middle_float, axis=1),
        ),
        "ep",
    )
    inv_second = lax.rsqrt(mid_squares / D + norm_eps)[:, None]
    dense_hidden = (jax.nn.silu(dense_pre * inv_second) * (dense_lin * inv_second)).astype(
        jnp.bfloat16
    )
    mix_gate = jax.nn.sigmoid(mix_pre * inv_second[:, 0])
    dense_part = (
        jnp.dot(dense_hidden, w_dense_down, preferred_element_type=jnp.float32) * mix_gate[:, None]
    )
    slot_count = CAP * ep_count
    expert_ids = (route_group[:, None] * EPG + route_inner).reshape(-1)
    expert_onehot = (expert_ids[:, None] == jnp.arange(EXPERTS, dtype=jnp.int32)[None, :]).astype(
        jnp.int32
    )
    per_block = expert_onehot.reshape(ep_count, seq_local * TOPK, EXPERTS)
    earlier = (jnp.cumsum(per_block, axis=1) - per_block).reshape(-1, EXPERTS)
    slot_rank = jnp.sum(earlier * expert_onehot, axis=1)
    route_index = jnp.arange(batch_all * TOPK, dtype=jnp.int32)
    block_of = route_index // (seq_local * TOPK)
    slot_flat = expert_ids * slot_count + block_of * CAP + slot_rank
    slot_table = (
        jnp.full((EXPERTS * slot_count,), batch_all, jnp.int32)
        .at[slot_flat]
        .set(route_index // TOPK)
    )
    padded_middle = jnp.concatenate([middle, jnp.zeros((1, col_width), jnp.bfloat16)], axis=0)
    outgoing = jnp.take(padded_middle, slot_table, axis=0).reshape(EXPERTS, slot_count, col_width)
    arrived_float = lax.all_to_all(outgoing, "ep", split_axis=0, concat_axis=2, tiled=True).astype(
        jnp.float32
    )
    inv_rows = lax.rsqrt(jnp.mean(arrived_float * arrived_float, axis=2, keepdims=True) + norm_eps)
    scaled_rows = (arrived_float * gain_float).astype(jnp.bfloat16)
    gate_pre = (
        jnp.einsum("end,edf->enf", scaled_rows, w_exp_gate, preferred_element_type=jnp.float32)
        * inv_rows
    )
    up_proj = (
        jnp.einsum("end,edf->enf", scaled_rows, w_exp_up, preferred_element_type=jnp.float32)
        * inv_rows
    )
    hidden = (jax.nn.silu(gate_pre) * up_proj).astype(jnp.bfloat16)
    expert_rows = jnp.einsum("enf,efd->end", hidden, w_exp_down, preferred_element_type=jnp.float32)
    returned = lax.all_to_all(expert_rows, "ep", split_axis=2, concat_axis=0, tiled=True)
    flat_back = returned.reshape(EXPERTS * slot_count, col_width)
    routed = jnp.take(flat_back, slot_flat, axis=0).reshape(batch_all, TOPK, col_width)
    expert_part = jnp.sum(routed * route_weight[:, :, None], axis=1)
    result_sum = middle_float + lax.psum(expert_part + dense_part, "tp")
    return (result_sum.astype(jnp.bfloat16), new_keys, new_values)


def solution(mesh):
    placed = (
        P(None, "ep"),
        P("ep"),
        P("ep", "tp"),
        P("ep", "tp"),
        P("ep", "tp"),
        P("tp", "ep"),
        P("ep", None, "tp"),
        P("ep", None, "tp"),
        P("ep"),
        P("tp"),
        P(),
        P("ep"),
        P("ep", "tp"),
        P("ep", "tp"),
        P("tp", "ep"),
        P(),
        P(),
        P(),
        P("ep", None, "tp"),
        P("ep", None, "tp"),
        P("ep", "tp", None),
    )
    return jax.shard_map(
        on_device,
        mesh=mesh,
        in_specs=placed,
        out_specs=(P(None, "ep"), P("ep", "tp"), P("ep", "tp")),
        check_vma=False,
    )
```

profile of v0, /device:TPU:0, one launch (start us, length us, event | category | flops | bytes accessed | tf_op | source)
XLA Modules:
  0.0 316.2 jit_solution(12506751394663622789)
XLA Ops:
  7.2 0.8 convert_element_type.69
  8.0 2.5 fusion.3
  10.6 1.0 fusion.14
  11.7 12.3 %copy.64 = bf16[16,1024,256]{1,2,0:T(8,128)(2,1)} copy(bf16[16,1024,256]{2,1,0:T(8,128)(2,1)} %param.27) | data formatting | bytes 16777216 | tf_op jit(solution)/shard_map/reshape | solution.py:65
  24.4 0.2 select_reduce_fusion
  24.8 0.1 mul.169
  24.9 0.6 dynamic-slice
  26.2 1.0 scatter_custom_fusion
  27.2 11.5 %all-reduce.1 = f32[64]{0:T(128)S(1)} all-reduce(f32[64]{0:T(128)S(1)} %fusion.14), channel_id=3, replica_groups=mesh['ep'=4,'tp'=8] {'ep'}, use_global_device_ids=true, to_apply=%region_2.0.clone | all-reduce | flops 64 | bytes 512
  38.8 0.9 multiply_convert_fusion.6
  39.7 0.6 fusion.57
  40.3 4.6 %fusion.58 = f32[16,2,1,1024]{3,2,1,0:T(1,128)S(1)} fusion(bf16[16,2,128,1]{2,3,1,0:T(2,128)(2,1)S(1)} %reshape.226, bf16[16,1024,2,128]{1,3,2,0:T(8,128)(2,1)} %bitcast.59), kind=kOutput, calls=%fused_computation.104 | convolution fusion | flops 8388608 | bytes 8527872 | tf_op jit(solution)/shard_map/bhd,blhd->bhl/dot_general | solution.py:66
  44.9 0.4 fusion.24
  45.4 39.6 %reduce-window.6 = f32[16,2,8,128]{3,2,1,0:T(8,128)S(1)} reduce-window(f32[16,2,8,128]{3,2,1,0:T(8,128)S(1)} %reshape.188, f32[]{:T(128)} %constant.94.clone.1), window={size=1x1x1x128 pad=0_0x0_0x0_0x0_127}, to_apply=%region_3.4 | reduce-window | flops 4161536 | bytes 262148 | tf_op jit(solution)/shard_map/reduce-window
  85.0 0.2 copy.48
  85.5 0.8 fusion.42
  86.4 4.6 %fusion = f32[16,2,1,128]{3,2,1,0:T(1,128)S(1)} fusion(bf16[16,2,1024,1]{2,1,0,3:T(2,128)(2,1)S(1)} %fusion.42, bf16[16,1024,256]{2,1,0:T(8,128)(2,1)} %param.28), kind=kOutput, calls=%fused_computation.3 | convolution fusion | flops 8388608 | bytes 8470528 | tf_op jit(solution)/shard_map/bhl,blhd->bhd/dot_general | solution.py:77
  91.0 7.1 %all_gather.3 = bf16[64,256]{1,0:T(8,128)(2,1)S(1)} all-gather(bf16[16,256]{1,0:T(8,128)(2,1)S(1)} %bitcast.70), channel_id=1, replica_groups=mesh['ep'=4,'tp'=8] {'ep'}, dimensions={0}, use_global_device_ids=true | all-gather | bytes 40960 | tf_op jit(solution)/shard_map/all_gather | solution.py:80
  98.1 0.9 fusion.59
  99.2 55.8 %all-reduce.8.cloned.1.call-done = f32[64,1024]{1,0:T(8,128)} async-done(((f32[64,1024]{1,0:T(8,128)}), f32[64,1024]{1,0:T(8,128)}) %all-reduce.8.cloned.1.call-update) | async-done | bytes 262160 | tf_op jit(solution)/shard_map/psum | solution.py:84
  154.9 1.1 fusion.17
  156.0 1.2 gather_fusion
  157.2 0.9 broadcast_select_fusion
  158.1 3.6 %all-to-all-start = ((bf16[16,16,1024]{2,1,0:T(8,128)(2,1)}), bf16[16,16,1024]{2,1,0:T(8,128)(2,1)S(1)}, u32[]{:S(2)}, u32[]{:S(2)}) async-start(bf16[16,16,1024]{2,1,0:T(8,128)(2,1)} %broadcast_select_fusion), calls=%async_computation.1 | async-start | bytes 1048576 | tf_op jit(solution)/shard_map/all_to_all | solution.py:125
  162.3 6.1 %all-to-all-done = bf16[16,16,1024]{2,1,0:T(8,128)(2,1)S(1)} async-done(((bf16[16,16,1024]{2,1,0:T(8,128)(2,1)}), bf16[16,16,1024]{2,1,0:T(8,128)(2,1)S(1)}, u32[]{:S(2)}, u32[]{:S(2)}) %all-to-all-start) | async-done | bytes 524320 | tf_op jit(solution)/shard_map/all_to_all | solution.py:125
  168.4 1.5 copy.82
  169.8 1.9 reshape.192
  171.8 0.2 multiply_reduce_fusion
  172.0 4.5 %convolution_multiply_fusion.2 = f32[4,16,256]{2,1,0:T(8,128)S(1)} fusion(bf16[4,4096,256]{2,1,0:T(8,128)(2,1)} %param.39, f32[4,16,4096]{2,1,0:T(8,128)S(1)} %reshape.192, f32[4096]{0:T(1024)S(1)} %convert_element_type.81, f32[4,16]{1,0:T(4,128)S(1)} %add_rsqrt_fusion), kind=kOutput, calls=%fused_computation.16 | convolution fusion | flops 134758400 | bytes 9519360 | tf_op jit(solution)/shard_map/end,edf->enf/dot_general | solution.py:131
  176.5 8.1 %fusion.12 = f32[4,16,4096]{2,1,0:T(8,128)S(1)} fusion(bf16[4,256,4096]{2,1,0:T(8,128)(2,1)} %param.41, bf16[4,4096,256]{2,1,0:T(8,128)(2,1)} %param.40, f32[4,16,4096]{2,1,0:T(8,128)S(1)} %reshape.192, f32[4096]{0:T(1024)S(1)} %convert_element_type.81, f32[4,16,256]{2,1,0:T(8,128)S(1)} %convolution_multiply_fusion.2, f32[4,16]{1,0:T(4,128)S(1)} %add_rsqrt_fusion), kind=kOutput, calls=%fused_computation.22 | convolution fusion | flops 269074432 | bytes 18956544 | tf_op jit(solution)/shard_map/enf,efd->end/dot_general | solution.py:139
  184.6 5.9 %copy.55 = f32[4,16,4096]{1,0,2:T(4,128)} copy(f32[4,16,4096]{2,1,0:T(8,128)S(1)} %fusion.12) | data formatting | bytes 2097152 | tf_op jit(solution)/shard_map/enf,efd->end/dot_general | solution.py:139
  190.5 8.8 %reshape.230 = f32[4,1,65536]{2,1,0:T(1,128)} reshape(f32[4096,4,16]{2,1,0:T(4,128)} %bitcast.60) | data formatting | bytes 2097152
  199.3 3.5 %all-to-all-start.1 = ((f32[4,1,65536]{2,1,0:T(1,128)}), f32[4,1,65536]{2,1,0:T(1,128)S(1)}, u32[]{:S(2)}, u32[]{:S(2)}) async-start(f32[4,1,65536]{2,1,0:T(1,128)} %reshape.230), calls=%async_computation.2 | async-start | bytes 2097152 | tf_op jit(solution)/shard_map/all_to_all | solution.py:140
  202.9 0.9 fusion.30
  203.8 2.2 fusion.32
  206.1 0.1 convolution_bitcast_fusion
  206.2 10.6 %all-reduce.2 = (f32[64]{0:T(128)S(1)}, f32[64]{0:T(128)S(1)}) all-reduce(f32[64]{0:T(128)S(1)} %convolution_bitcast_fusion, f32[64]{0:T(128)S(1)} %get-tuple-element.7), channel_id=1, replica_groups=mesh['ep'=4,'tp'=8] {'ep'}, use_global_device_ids=true, to_apply=%region_16.17 | all-reduce | flops 128 | bytes 1024 | tf_op jit(solution)/shard_map/psum | solution.py:90
  216.9 0.6 broadcast.214
  217.5 3.7 %reduce.5 = f32[4,65536]{1,0:T(4,128)S(1)} reduce(f32[4,1,65536]{2,1,0:T(1,128)S(1)} %all-to-all-done.1, f32[]{:T(128)} %broadcast.214), dimensions={1}, to_apply=%all_to_all.9.reduce_sub_computation | reduce | bytes 2097156 | tf_op jit(solution)/shard_map/all_to_all | solution.py:140
  221.2 9.1 %reshape.231 = f32[4096,4,16]{2,1,0:T(4,128)} reshape(f32[4,65536]{1,0:T(4,128)S(1)} %reduce.5) | data formatting | bytes 2097152
  230.3 6.7 %copy.56 = f32[4,16,4,1024]{3,1,0,2:T(8,128)S(1)} copy(f32[4,16,4,1024]{1,0,3,2:T(4,128)} %bitcast.61) | data formatting | bytes 2097152 | tf_op jit(solution)/shard_map/all_to_all | solution.py:140
  236.9 0.8 gather_fusion.1
  237.7 0.3 gather.15
  238.1 0.8 multiply_reduce_fusion.1
  238.9 11.5 %all-reduce.12.cloned.1.call-done = (f32[64,512]{1,0:T(8,128)}, f32[64,512]{1,0:T(8,128)}) async-done(((f32[64,512]{1,0:T(8,128)}, f32[64,512]{1,0:T(8,128)}), (f32[64,512]{1,0:T(8,128)}, f32[64,512]{1,0:T(8,128)})) %all-reduce.12.cloned.1.call-update) | async-done | bytes 262160 | tf_op jit(solution)/shard_map/psum | solution.py:90
  250.4 2.0 fusion.9
  252.5 55.6 %all-reduce.10.cloned.1.call-done = f32[64,1024]{1,0:T(8,128)} async-done(((f32[64,1024]{1,0:T(8,128)}), f32[64,1024]{1,0:T(8,128)}) %all-reduce.10.cloned.1.call-update) | async-done | bytes 262160 | tf_op jit(solution)/shard_map/psum | solution.py:144
  308.1 1.6 fusion.18
  (71 shorter events, 1.9 us)
Async XLA Ops:
  7.2 243.3 %copy-start = (bf16[512,1024]{1,0:T(8,128)(2,1)S(1)}, bf16[512,1024]{1,0:T(8,128)(2,1)}, u32[]{:S(2)}) copy-start(bf16[512,1024]{1,0:T(8,128)(2,1)} %param.35) | copy-start | bytes 3145732
  7.2 31.6 %reduce-scatter.2.cloned.1.call-start = ((), (), s32[]{:S(2)}) async-start(), calls=%async_computation.3 | async-start | bytes 245760 | tf_op jit(solution)/shard_map/reduce_scatter | solution.py:52
  10.5 144.4 %all-reduce.8.cloned.1.call-start = ((), (), s32[]{:S(2)}) async-start(), calls=%async_computation.4 | async-start | bytes 524288 | tf_op jit(solution)/shard_map/psum | solution.py:84
  11.6 12.3 %copy-start.10 = (s32[64]{0:T(128)S(1)}, s32[64]{0:T(128)}, u32[]{:S(2)}) copy-start(s32[64]{0:T(128)} %param.36) | copy-start | bytes 772
  11.6 12.3 %copy-start.8 = (s32[64,2]{0,1:T(2,128)S(1)}, s32[64,2]{0,1:T(2,128)}, u32[]{:S(2)}) copy-start(s32[64,2]{0,1:T(2,128)} %param.37) | copy-start | bytes 1540
  11.6 13.3 %copy-start.11 = (u32[32]{0:T(128)S(1)}, u32[32]{0:T(128)}, u32[]{:S(2)}) copy-start(u32[32]{0:T(128)} %constant.122) | copy-start | bytes 388
  24.0 20.9 %copy-start.5 = (s32[16]{0:T(128)S(1)}, s32[16]{0:T(128)}, u32[]{:S(2)}) copy-start(s32[16]{0:T(128)} %param.29) | copy-start | bytes 196
  24.0 20.9 %copy-start.6 = (f32[2]{0:T(128)S(1)}, f32[2]{0:T(128)}, u32[]{:S(2)}) copy-start(f32[2]{0:T(128)} %param.30) | copy-start | bytes 28
  44.9 53.3 %copy-start.3 = (bf16[256,1024]{1,0:T(8,128)(2,1)S(1)}, bf16[256,1024]{1,0:T(8,128)(2,1)}, u32[]{:S(2)}) copy-start(bf16[256,1024]{1,0:T(8,128)(2,1)} %param.26) | copy-start | bytes 1572868
  44.9 110.1 %copy-start.2 = (bf16[64,1024]{1,0:T(8,128)(2,1)S(1)}, bf16[64,1024]{1,0:T(8,128)(2,1)}, u32[]{:S(2)}) copy-start(bf16[64,1024]{1,0:T(8,128)(2,1)} %param.21) | copy-start | bytes 393220
  86.3 75.5 %copy-start.4 = (bf16[4096]{0:T(1024)(128)(2,1)S(1)}, bf16[4096]{0:T(1024)(128)(2,1)}, u32[]{:S(2)}) copy-start(bf16[4096]{0:T(1024)(128)(2,1)} %param.31) | copy-start | bytes 24580
  86.4 75.8 %copy-start.9 = (f32[64,2]{0,1:T(2,128)S(1)}, f32[64,2]{0,1:T(2,128)}, u32[]{:S(2)}) copy-start(f32[64,2]{0,1:T(2,128)} %param.38) | copy-start | bytes 1540
  86.4 75.8 %copy-start.7 = (bf16[1024]{0:T(1024)(128)(2,1)S(1)}, bf16[1024]{0:T(1024)(128)(2,1)}, u32[]{:S(2)}) copy-start(bf16[1024]{0:T(1024)(128)(2,1)} %param.32) | copy-start | bytes 6148
  158.1 10.3 %all-to-all-start = ((bf16[16,16,1024]{2,1,0:T(8,128)(2,1)}), bf16[16,16,1024]{2,1,0:T(8,128)(2,1)S(1)}, u32[]{:S(2)}, u32[]{:S(2)}) async-start(bf16[16,16,1024]{2,1,0:T(8,128)(2,1)} %broadcast_select_fusion), calls=%async_computation.1 | async-start | bytes 1048576 | tf_op jit(solution)/shard_map/all_to_all | solution.py:125
  184.6 18.2 %copy-start.1 = (bf16[1024,512]{1,0:T(8,128)(2,1)S(1)}, bf16[1024,512]{1,0:T(8,128)(2,1)}, u32[]{:S(2)}) copy-start(bf16[1024,512]{1,0:T(8,128)(2,1)} %param.34) | copy-start | bytes 3145732
  199.3 17.6 %all-to-all-start.1 = ((f32[4,1,65536]{2,1,0:T(1,128)}), f32[4,1,65536]{2,1,0:T(1,128)S(1)}, u32[]{:S(2)}, u32[]{:S(2)}) async-start(f32[4,1,65536]{2,1,0:T(1,128)} %reshape.230), calls=%async_computation.2 | async-start | bytes 2097152 | tf_op jit(solution)/shard_map/all_to_all | solution.py:140
  202.8 47.6 %all-reduce.12.cloned.1.call-start = ((), (), s32[]{:S(2)}) async-start(), calls=%async_computation.6 | async-start | bytes 524288 | tf_op jit(solution)/shard_map/psum | solution.py:90
  206.0 102.0 %all-reduce.10.cloned.1.call-start = ((), (), s32[]{:S(2)}) async-start(), calls=%async_computation.5 | async-start | bytes 524288 | tf_op jit(solution)/shard_map/psum | solution.py:144
Sparse Core Ops, SparseCore 0:
  10.7 26.9 reduce-scatter.1
  99.2 55.6 all-reduce.7
  207.1 43.2 all-reduce.11
  252.6 55.4 all-reduce.9
where the time goes:
time: 317 us; the launch traced here: 316 us
  waiting for transfers between devices  129 us (41%)
  local copies, waits for them, and re-layouts  52.7 us (17%)
  other arithmetic  52.6 us (17%)
  matrix products  30.5 us (10%)
  blocking collectives  29.3 us (9%)
  between operations  14.8 us (5%)
  starting transfers between devices  7.33 us (2%)
    psum x1, waiting for transfers between devices, on_device(): attn_out = lax.psum(attn_part, 'tp')  55.8 us
    psum x1, waiting for transfers between devices, on_device(): result_sum = middle_float + lax.psum(expert_part + dense_part, 'tp')  55.6 us
    another operation x3, other arithmetic  40.5 us
    unnamed x30, local copies, waits for them, and re-layouts  18.6 us
    reshape x1, local copies, waits for them, and re-layouts, on_device(): head_keys = key_cache.reshape(seq_local, cache_len, heads_local, HD)  12.3 us
    psum x1, waiting for transfers between devices, on_device(): lax.psum((jnp.dot(scaled_mid, w_dense_gate, preferred_element_type=jnp.fl...  11.5 us
    unnamed x1, blocking collectives  11.5 us
    psum x1, blocking collectives, on_device(): lax.psum((jnp.dot(scaled_mid, w_dense_gate, preferred_element_type=jnp.fl...  10.6 us
  transfers between devices with their start and end apart: 6, of which 4 were waited for; matrix products, arithmetic and copies ran while one was open for 13% of the time, Pallas kernels for 0%

commit v1 on v0

--- a/solution.py
+++ b/solution.py
@@ -141,7 +141,8 @@
     flat_back = returned.reshape(EXPERTS * slot_count, col_width)
     routed = jnp.take(flat_back, slot_flat, axis=0).reshape(batch_all, TOPK, col_width)
     expert_part = jnp.sum(routed * route_weight[:, :, None], axis=1)
-    result_sum = middle_float + lax.psum(expert_part + dense_part, "tp")
+    play_spot = lambda matrix: lax.all_gather(matrix, "tp").sum(axis=0)
+    result_sum = middle_float + play_spot(expert_part + dense_part)
     return (result_sum.astype(jnp.bfloat16), new_keys, new_values)
 
 

time: 317 us -> 292 us (0.921)
  waiting for transfers between devices: 129 us -> 103 us
    psum x1 -> x0, waiting for transfers between devices: 55.6 us -> none  [on_device(): result_sum = middle_float + lax.psum(expert_part + dense_part, 'tp')]
    all_gather x0 -> x1, waiting for transfers between devices: none -> 29.3 us  [on_device(): play_spot = lambda matrix: lax.all_gather(matrix, 'tp').sum(axis=0)]
  transfers between devices with their start and end apart: 6 -> 6, of which waited for: 4 -> 4; matrix products, arithmetic and copies ran while one was open for 13% -> 14% of each run, Pallas kernels for 0% -> 0%
where the time goes in v1:
time: 292 us; the launch traced here: 291 us
  waiting for transfers between devices  103 us (35%)
  other arithmetic  53.4 us (18%)
  local copies, waits for them, and re-layouts  52.7 us (18%)
  matrix products  30.5 us (10%)
  blocking collectives  29.3 us (10%)
  between operations  14.8 us (5%)
  starting transfers between devices  7.33 us (3%)
    psum x1, waiting for transfers between devices, on_device(): attn_out = lax.psum(attn_part, 'tp')  55.8 us
    another operation x3, other arithmetic  40.5 us
    all_gather x1, waiting for transfers between devices, on_device(): play_spot = lambda matrix: lax.all_gather(matrix, 'tp').sum(axis=0)  29.3 us
    unnamed x30, local copies, waits for them, and re-layouts  18.6 us
    reshape x1, local copies, waits for them, and re-layouts, on_device(): head_keys = key_cache.reshape(seq_local, cache_len, heads_local, HD)  12.3 us
    psum x1, waiting for transfers between devices, on_device(): lax.psum((jnp.dot(scaled_mid, w_dense_gate, preferred_element_type=jnp.fl...  11.5 us
    unnamed x1, blocking collectives  11.5 us
    psum x1, blocking collectives, on_device(): lax.psum((jnp.dot(scaled_mid, w_dense_gate, preferred_element_type=jnp.fl...  10.6 us
  transfers between devices with their start and end apart: 6, of which 4 were waited for; matrix products, arithmetic and copies ran while one was open for 14% of the time, Pallas kernels for 0%

profile of v1, /device:TPU:0, one launch (start us, length us, event | category | flops | bytes accessed | tf_op | source)
XLA Modules:
  0.0 290.8 jit_solution(15931744669442809345)
XLA Ops:
  7.2 0.8 convert_element_type.69
  8.0 2.5 fusion.3
  10.6 1.0 fusion.14
  11.7 12.3 %copy.64 = bf16[16,1024,256]{1,2,0:T(8,128)(2,1)} copy(bf16[16,1024,256]{2,1,0:T(8,128)(2,1)} %param.27) | data formatting | bytes 16777216 | tf_op jit(solution)/shard_map/reshape | solution.py:65
  24.4 0.2 select_reduce_fusion
  24.8 0.1 mul.169
  24.9 0.6 dynamic-slice
  26.2 1.0 scatter_custom_fusion
  27.2 11.5 %all-reduce.1 = f32[64]{0:T(128)S(1)} all-reduce(f32[64]{0:T(128)S(1)} %fusion.14), channel_id=4, replica_groups=mesh['ep'=4,'tp'=8] {'ep'}, use_global_device_ids=true, to_apply=%region_2.0.clone | all-reduce | flops 64 | bytes 512
  38.8 0.9 multiply_convert_fusion.6
  39.7 0.6 fusion.57
  40.3 4.6 %fusion.58 = f32[16,2,1,1024]{3,2,1,0:T(1,128)S(1)} fusion(bf16[16,2,128,1]{2,3,1,0:T(2,128)(2,1)S(1)} %reshape.227, bf16[16,1024,2,128]{1,3,2,0:T(8,128)(2,1)} %bitcast.60), kind=kOutput, calls=%fused_computation.104 | convolution fusion | flops 8388608 | bytes 8527872 | tf_op jit(solution)/shard_map/bhd,blhd->bhl/dot_general | solution.py:66
  44.9 0.4 fusion.24
  45.4 39.6 %reduce-window.6 = f32[16,2,8,128]{3,2,1,0:T(8,128)S(1)} reduce-window(f32[16,2,8,128]{3,2,1,0:T(8,128)S(1)} %reshape.188, f32[]{:T(128)} %constant.94.clone.1), window={size=1x1x1x128 pad=0_0x0_0x0_0x0_127}, to_apply=%region_3.4 | reduce-window | flops 4161536 | bytes 262148 | tf_op jit(solution)/shard_map/reduce-window
  85.0 0.2 copy.48
  85.5 0.8 fusion.42
  86.4 4.6 %fusion = f32[16,2,1,128]{3,2,1,0:T(1,128)S(1)} fusion(bf16[16,2,1024,1]{2,1,0,3:T(2,128)(2,1)S(1)} %fusion.42, bf16[16,1024,256]{2,1,0:T(8,128)(2,1)} %param.28), kind=kOutput, calls=%fused_computation.3 | convolution fusion | flops 8388608 | bytes 8470528 | tf_op jit(solution)/shard_map/bhl,blhd->bhd/dot_general | solution.py:77
  91.0 7.1 %all_gather.9 = bf16[64,256]{1,0:T(8,128)(2,1)S(1)} all-gather(bf16[16,256]{1,0:T(8,128)(2,1)S(1)} %bitcast.72), channel_id=1, replica_groups=mesh['ep'=4,'tp'=8] {'ep'}, dimensions={0}, use_global_device_ids=true | all-gather | bytes 40960 | tf_op jit(solution)/shard_map/all_gather | solution.py:80
  98.1 0.9 fusion.59
  99.2 55.8 %all-reduce.7.cloned.1.call-done = f32[64,1024]{1,0:T(8,128)} async-done(((f32[64,1024]{1,0:T(8,128)}), f32[64,1024]{1,0:T(8,128)}) %all-reduce.7.cloned.1.call-update) | async-done | bytes 262160 | tf_op jit(solution)/shard_map/psum | solution.py:84
  154.9 1.1 fusion.17
  156.0 1.2 gather_fusion
  157.2 0.9 broadcast_select_fusion
  158.1 3.6 %all-to-all-start = ((bf16[16,16,1024]{2,1,0:T(8,128)(2,1)}), bf16[16,16,1024]{2,1,0:T(8,128)(2,1)S(1)}, u32[]{:S(2)}, u32[]{:S(2)}) async-start(bf16[16,16,1024]{2,1,0:T(8,128)(2,1)} %broadcast_select_fusion), calls=%async_computation.1 | async-start | bytes 1048576 | tf_op jit(solution)/shard_map/all_to_all | solution.py:125
  162.3 6.1 %all-to-all-done = bf16[16,16,1024]{2,1,0:T(8,128)(2,1)S(1)} async-done(((bf16[16,16,1024]{2,1,0:T(8,128)(2,1)}), bf16[16,16,1024]{2,1,0:T(8,128)(2,1)S(1)}, u32[]{:S(2)}, u32[]{:S(2)}) %all-to-all-start) | async-done | bytes 524320 | tf_op jit(solution)/shard_map/all_to_all | solution.py:125
  168.4 1.5 copy.82
  169.8 1.9 reshape.192
  171.8 0.2 multiply_reduce_fusion
  172.0 4.5 %convolution_multiply_fusion.2 = f32[4,16,256]{2,1,0:T(8,128)S(1)} fusion(bf16[4,4096,256]{2,1,0:T(8,128)(2,1)} %param.39, f32[4,16,4096]{2,1,0:T(8,128)S(1)} %reshape.192, f32[4096]{0:T(1024)S(1)} %convert_element_type.81, f32[4,16]{1,0:T(4,128)S(1)} %add_rsqrt_fusion), kind=kOutput, calls=%fused_computation.16 | convolution fusion | flops 134758400 | bytes 9519360 | tf_op jit(solution)/shard_map/end,edf->enf/dot_general | solution.py:131
  176.5 8.1 %fusion.12 = f32[4,16,4096]{2,1,0:T(8,128)S(1)} fusion(bf16[4,256,4096]{2,1,0:T(8,128)(2,1)} %param.41, bf16[4,4096,256]{2,1,0:T(8,128)(2,1)} %param.40, f32[4,16,4096]{2,1,0:T(8,128)S(1)} %reshape.192, f32[4096]{0:T(1024)S(1)} %convert_element_type.81, f32[4,16,256]{2,1,0:T(8,128)S(1)} %convolution_multiply_fusion.2, f32[4,16]{1,0:T(4,128)S(1)} %add_rsqrt_fusion), kind=kOutput, calls=%fused_computation.22 | convolution fusion | flops 269074432 | bytes 18956544 | tf_op jit(solution)/shard_map/enf,efd->end/dot_general | solution.py:139
  184.6 5.9 %copy.55 = f32[4,16,4096]{1,0,2:T(4,128)} copy(f32[4,16,4096]{2,1,0:T(8,128)S(1)} %fusion.12) | data formatting | bytes 2097152 | tf_op jit(solution)/shard_map/enf,efd->end/dot_general | solution.py:139
  190.5 8.8 %reshape.231 = f32[4,1,65536]{2,1,0:T(1,128)} reshape(f32[4096,4,16]{2,1,0:T(4,128)} %bitcast.61) | data formatting | bytes 2097152
  199.3 3.5 %all-to-all-start.1 = ((f32[4,1,65536]{2,1,0:T(1,128)}), f32[4,1,65536]{2,1,0:T(1,128)S(1)}, u32[]{:S(2)}, u32[]{:S(2)}) async-start(f32[4,1,65536]{2,1,0:T(1,128)} %reshape.231), calls=%async_computation.2 | async-start | bytes 2097152 | tf_op jit(solution)/shard_map/all_to_all | solution.py:140
  202.9 0.9 fusion.30
  203.8 2.2 fusion.32
  206.2 10.6 %all-reduce.2 = (f32[64]{0:T(128)S(1)}, f32[64]{0:T(128)S(1)}) all-reduce(f32[64]{0:T(128)S(1)} %convolution_bitcast_fusion, f32[64]{0:T(128)S(1)} %get-tuple-element.7), channel_id=1, replica_groups=mesh['ep'=4,'tp'=8] {'ep'}, use_global_device_ids=true, to_apply=%region_16.17 | all-reduce | flops 128 | bytes 1024 | tf_op jit(solution)/shard_map/psum | solution.py:90
  216.9 0.6 broadcast.214
  217.5 3.7 %reduce.5 = f32[4,65536]{1,0:T(4,128)S(1)} reduce(f32[4,1,65536]{2,1,0:T(1,128)S(1)} %all-to-all-done.1, f32[]{:T(128)} %broadcast.214), dimensions={1}, to_apply=%all_to_all.9.reduce_sub_computation | reduce | bytes 2097156 | tf_op jit(solution)/shard_map/all_to_all | solution.py:140
  221.2 9.1 %reshape.232 = f32[4096,4,16]{2,1,0:T(4,128)} reshape(f32[4,65536]{1,0:T(4,128)S(1)} %reduce.5) | data formatting | bytes 2097152
  230.3 6.7 %copy.56 = f32[4,16,4,1024]{3,1,0,2:T(8,128)S(1)} copy(f32[4,16,4,1024]{1,0,3,2:T(4,128)} %bitcast.62) | data formatting | bytes 2097152 | tf_op jit(solution)/shard_map/all_to_all | solution.py:140
  236.9 0.8 gather_fusion.1
  237.7 0.3 gather.15
  238.1 0.8 multiply_reduce_fusion.1
  238.9 11.5 %all-reduce.9.cloned.1.call-done = (f32[64,512]{1,0:T(8,128)}, f32[64,512]{1,0:T(8,128)}) async-done(((f32[64,512]{1,0:T(8,128)}, f32[64,512]{1,0:T(8,128)}), (f32[64,512]{1,0:T(8,128)}, f32[64,512]{1,0:T(8,128)})) %all-reduce.9.cloned.1.call-update) | async-done | bytes 262160 | tf_op jit(solution)/shard_map/psum | solution.py:90
  250.4 2.1 fusion.9
  252.5 29.3 %all-gather.3.cloned.1.call-done = f32[512,1024]{1,0:T(8,128)} async-done(((f32[64,1024]{1,0:T(8,128)}), f32[512,1024]{1,0:T(8,128)}) %all-gather.3.cloned.1.call-update) | async-done | bytes 2097168 | tf_op jit(solution)/shard_map/all_gather | solution.py:144
  281.8 1.7 reduce_sum.74
  283.6 0.7 fusion.18
  (72 shorter events, 2.1 us)
Async XLA Ops:
  7.2 243.3 %copy-start = (bf16[512,1024]{1,0:T(8,128)(2,1)S(1)}, bf16[512,1024]{1,0:T(8,128)(2,1)}, u32[]{:S(2)}) copy-start(bf16[512,1024]{1,0:T(8,128)(2,1)} %param.35) | copy-start | bytes 3145732
  7.2 31.6 %reduce-scatter.2.cloned.1.call-start = ((), (), s32[]{:S(2)}) async-start(), calls=%async_computation.3 | async-start | bytes 245760 | tf_op jit(solution)/shard_map/reduce_scatter | solution.py:52
  10.5 144.4 %all-reduce.7.cloned.1.call-start = ((), (), s32[]{:S(2)}) async-start(), calls=%async_computation.4 | async-start | bytes 524288 | tf_op jit(solution)/shard_map/psum | solution.py:84
  11.6 12.3 %copy-start.10 = (s32[64]{0:T(128)S(1)}, s32[64]{0:T(128)}, u32[]{:S(2)}) copy-start(s32[64]{0:T(128)} %param.36) | copy-start | bytes 772
  11.6 12.3 %copy-start.8 = (s32[64,2]{0,1:T(2,128)S(1)}, s32[64,2]{0,1:T(2,128)}, u32[]{:S(2)}) copy-start(s32[64,2]{0,1:T(2,128)} %param.37) | copy-start | bytes 1540
  11.6 13.3 %copy-start.11 = (u32[32]{0:T(128)S(1)}, u32[32]{0:T(128)}, u32[]{:S(2)}) copy-start(u32[32]{0:T(128)} %constant.122) | copy-start | bytes 388
  24.0 20.9 %copy-start.5 = (s32[16]{0:T(128)S(1)}, s32[16]{0:T(128)}, u32[]{:S(2)}) copy-start(s32[16]{0:T(128)} %param.29) | copy-start | bytes 196
  24.0 20.9 %copy-start.6 = (f32[2]{0:T(128)S(1)}, f32[2]{0:T(128)}, u32[]{:S(2)}) copy-start(f32[2]{0:T(128)} %param.30) | copy-start | bytes 28
  44.9 53.3 %copy-start.3 = (bf16[256,1024]{1,0:T(8,128)(2,1)S(1)}, bf16[256,1024]{1,0:T(8,128)(2,1)}, u32[]{:S(2)}) copy-start(bf16[256,1024]{1,0:T(8,128)(2,1)} %param.26) | copy-start | bytes 1572868
  44.9 110.1 %copy-start.2 = (bf16[64,1024]{1,0:T(8,128)(2,1)S(1)}, bf16[64,1024]{1,0:T(8,128)(2,1)}, u32[]{:S(2)}) copy-start(bf16[64,1024]{1,0:T(8,128)(2,1)} %param.21) | copy-start | bytes 393220
  86.3 75.5 %copy-start.4 = (bf16[4096]{0:T(1024)(128)(2,1)S(1)}, bf16[4096]{0:T(1024)(128)(2,1)}, u32[]{:S(2)}) copy-start(bf16[4096]{0:T(1024)(128)(2,1)} %param.31) | copy-start | bytes 24580
  86.4 75.8 %copy-start.9 = (f32[64,2]{0,1:T(2,128)S(1)}, f32[64,2]{0,1:T(2,128)}, u32[]{:S(2)}) copy-start(f32[64,2]{0,1:T(2,128)} %param.38) | copy-start | bytes 1540
  86.4 75.8 %copy-start.7 = (bf16[1024]{0:T(1024)(128)(2,1)S(1)}, bf16[1024]{0:T(1024)(128)(2,1)}, u32[]{:S(2)}) copy-start(bf16[1024]{0:T(1024)(128)(2,1)} %param.32) | copy-start | bytes 6148
  158.1 10.3 %all-to-all-start = ((bf16[16,16,1024]{2,1,0:T(8,128)(2,1)}), bf16[16,16,1024]{2,1,0:T(8,128)(2,1)S(1)}, u32[]{:S(2)}, u32[]{:S(2)}) async-start(bf16[16,16,1024]{2,1,0:T(8,128)(2,1)} %broadcast_select_fusion), calls=%async_computation.1 | async-start | bytes 1048576 | tf_op jit(solution)/shard_map/all_to_all | solution.py:125
  184.6 18.2 %copy-start.1 = (bf16[1024,512]{1,0:T(8,128)(2,1)S(1)}, bf16[1024,512]{1,0:T(8,128)(2,1)}, u32[]{:S(2)}) copy-start(bf16[1024,512]{1,0:T(8,128)(2,1)} %param.34) | copy-start | bytes 3145732
  199.3 17.6 %all-to-all-start.1 = ((f32[4,1,65536]{2,1,0:T(1,128)}), f32[4,1,65536]{2,1,0:T(1,128)S(1)}, u32[]{:S(2)}, u32[]{:S(2)}) async-start(f32[4,1,65536]{2,1,0:T(1,128)} %reshape.231), calls=%async_computation.2 | async-start | bytes 2097152 | tf_op jit(solution)/shard_map/all_to_all | solution.py:140
  202.8 47.6 %all-reduce.9.cloned.1.call-start = ((), (), s32[]{:S(2)}) async-start(), calls=%async_computation.6 | async-start | bytes 524288 | tf_op jit(solution)/shard_map/psum | solution.py:90
  206.0 75.8 %all-gather.3.cloned.1.call-start = ((), (), s32[]{:S(2)}) async-start(), calls=%async_computation.5 | async-start | bytes 2359296 | tf_op jit(solution)/shard_map/all_gather | solution.py:144
Sparse Core Ops, SparseCore 0:
  10.7 26.9 reduce-scatter.1
  99.2 55.6 all-reduce.6
  207.1 43.2 all-reduce.8
  252.6 29.1 all-gather.2
